TPU v7x, 32 devices: a whole 2x2x4 slice. The times are simulated.
32 devices in a mesh: sp: 8 (over z, core), tp: 4 (over y, x).
Axes of the slice: x: 2, y: 2, z: 4, core: 2. Of those that a mesh axis runs over, the one named last changes fastest.
Arguments:
- query_heads: bfloat16 [2048, 1024], P('sp', 'tp'), may hold values from -6 to 6
- key_heads: bfloat16 [2048, 256], P('sp'), may hold values from -6 to 6
- value_heads: bfloat16 [2048, 256], P('sp'), may hold values from -24 to 24
- q_gain: float32 [64], replicated, may hold values from 0.6 to 4.5
- k_gain: float32 [64], replicated, may hold values from 0.6 to 4.5
- out_weight: bfloat16 [1024, 2048], P('tp'), may hold values from -0.1875 to 0.1875
- residual: bfloat16 [2048, 2048], P('sp', 'tp'), may hold values from -3 to 3
- norm_gain: float32 [2048], P('tp'), may hold values from 0.1 to 1.9
- routes: int32 [2048, 2], P('sp'), may hold values from 0 to 7, all different within a row; in each aligned block of 256 rows (0 to 255, 256 to 511, ...) at most 81 rows name the same one
- route_weights: float32 [2048, 2], P('sp'), may hold values from 0.5 to 1.5
- w_gate: bfloat16 [8, 2048, 4096], P('sp', None, 'tp'), may hold values from -0.125 to 0.125
- w_up: bfloat16 [8, 2048, 4096], P('sp', None, 'tp'), may hold values from -0.125 to 0.125
- w_down: bfloat16 [8, 4096, 2048], P('sp', 'tp'), may hold values from -0.1875 to 0.1875
Outputs:
- layer_out: bfloat16 [2048, 2048], P('sp', 'tp')
Inputs may be any that keep to these rules, and one draw needn't show every extreme that they name: `routes`: each row names 2 different experts. Among the 256 rows of one index of sp, no expert is named more than 81 times, a bound that some block reaches.
All inputs are finite; a program needn't handle non-finite values.
Results may differ from a plain program's by a relative error of at most 0.02.
The roundings to bfloat16 on the way count: a program that leaves them out, or rounds other values in their place, can miss the bound.
Values may be sent and summed in bfloat16 or wider, within the bound.
A program may use at most 64 MiB of HBM per device.

v0:
```python
import functools

import jax
import jax.numpy as jnp
import numpy as np
from jax import lax
from jax.experimental import pallas as pl
from jax.experimental.pallas import tpu as pltpu
from jax.sharding import PartitionSpec as P

D = 2048
HQ = 16
KV = 4
E = 64
TOPK = 2
GRID_W = 64

norm_eps = 1e-06
rope_base = 10000.0

MESH = pl.DeviceIdType.MESH
VMEM = pltpu.VMEM
F32 = jnp.float32
BF16 = jnp.bfloat16
ROW_TILE = 8


def normalize(values_f, gain):
    mean_sq = jnp.mean(values_f * values_f, axis=-1, keepdims=True)
    return values_f * lax.rsqrt(mean_sq + norm_eps) * gain


def rotate(values_f, positions):
    head_width = values_f.shape[-1]
    half_width = head_width // 2
    quarter_width = half_width // 2
    frequency = rope_base ** (-jnp.arange(quarter_width, dtype=jnp.float32) / quarter_width)
    grid_rows = (positions // GRID_W).astype(jnp.float32)
    grid_cols = (positions % GRID_W).astype(jnp.float32)
    shape = (values_f.shape[0],) + (1,) * (values_f.ndim - 2) + (quarter_width,)
    pieces = []
    for coords, offset_lo in ((grid_rows, 0), (grid_cols, half_width)):
        angles = coords[:, None] * frequency[None, :]
        cosine = jnp.cos(angles).reshape(shape)
        sines = jnp.sin(angles).reshape(shape)
        first_part = values_f[..., offset_lo : offset_lo + quarter_width]
        second_part = values_f[..., offset_lo + quarter_width : offset_lo + half_width]
        pieces.append(first_part * cosine - second_part * sines)
        pieces.append(second_part * cosine + first_part * sines)
    return jnp.concatenate(pieces, axis=-1)


def dot(a, b):
    return jnp.dot(a, b, preferred_element_type=F32)


def tp_offset(tp, n_tp, q):
    if n_tp == 4:
        x = lax.rem(lax.rem(tp, 2) + q % 2, 2)
        y = lax.rem(lax.div(tp, 2) + q // 2, 2)
        return y * 2 + x
    return lax.rem(tp + q, n_tp)


def tp_origin(tp, n_tp, q):
    return tp_offset(tp, n_tp, q if n_tp == 4 else n_tp - q)


def remote(src, dst, send_sem, recv_sem, sp, tp):
    return pltpu.make_async_remote_copy(
        src_ref=src, dst_ref=dst, send_sem=send_sem, recv_sem=recv_sem,
        device_id=(sp, tp), device_id_type=MESH,
    )


def gather_kernel(
    n_sp, n_tp, own, weight, out, weight_out, send, recv, send2, recv2, w_send, w_recv,
    v_send, v_recv
):
    me = lax.axis_index("sp")
    tp = lax.axis_index("tp")
    chips = n_sp // 2
    core = lax.rem(me, 2)
    z = lax.div(me, 2)
    partner = z * 2 + 1 - core
    barrier = pltpu.get_barrier_semaphore()
    pl.semaphore_signal(barrier, inc=1, device_id=(partner, tp), device_id_type=MESH)
    for j in range(1, chips):
        pl.semaphore_signal(
            barrier, inc=1, device_id=(lax.rem(z + j, chips) * 2 + core, tp), device_id_type=MESH
        )
    for q in range(1, n_tp):
        pl.semaphore_signal(
            barrier, inc=1, device_id=(me, tp_offset(tp, n_tp, q)), device_id_type=MESH
        )
    pl.semaphore_wait(barrier, chips + n_tp - 1)
    first = []
    for j in range(1, chips):
        copy = remote(own, out.at[me], send.at[j], recv.at[j], lax.rem(z + j, chips) * 2 + core, tp)
        copy.start()
        first.append(copy)
    swap = remote(own, out.at[me], send2.at[0], recv2.at[0], partner, tp)
    swap.start()
    out[me] = own[...]
    cols = weight_out.shape[2]
    depth = weight.shape[0] // 2
    mine = pl.ds(pl.multiple_of(core * depth, 16), depth)
    third = {}
    for q in range(n_tp - 1, 0, -1):
        peer = tp_offset(tp, n_tp, q)
        part = weight.at[mine, pl.ds(pl.multiple_of(peer * cols, 128), cols)]
        third[q] = remote(
            part, weight_out.at[tp, mine, :], w_send.at[q], w_recv.at[q], me, peer
        )
        third[q].start()
    weight_out[tp] = weight[:, pl.ds(pl.multiple_of(tp * cols, 128), cols)]
    second = [swap]
    for j in range(1, chips):
        first[j - 1].wait_recv()
        source = lax.rem(z + chips - j, chips) * 2 + core
        copy = remote(out.at[source], out.at[source], send2.at[j], recv2.at[j], partner, tp)
        copy.start()
        second.append(copy)
    for q in range(1, n_tp):
        third[q].wait_recv()
        part = weight_out.at[tp_origin(tp, n_tp, q), mine, :]
        copy = remote(part, part, v_send.at[q], v_recv.at[q], partner, tp)
        copy.start()
        second.append(copy)
    for copy in second:
        copy.wait()
    for copy in first + list(third.values()):
        copy.wait_send()


def gather_kv(n_sp, n_tp, own, weight):
    rows, width = own.shape
    depth, feats = weight.shape
    return pl.pallas_call(
        functools.partial(gather_kernel, n_sp, n_tp),
        out_shape=(
            jax.ShapeDtypeStruct((n_sp, rows, width), own.dtype),
            jax.ShapeDtypeStruct((n_tp, depth, feats // n_tp), weight.dtype),
        ),
        in_specs=[pl.BlockSpec(memory_space=VMEM)] * 2,
        out_specs=[pl.BlockSpec(memory_space=VMEM)] * 2,
        scratch_shapes=[pltpu.SemaphoreType.DMA((n_sp // 2,))] * 4
        + [pltpu.SemaphoreType.DMA((n_tp,))] * 4,
        compiler_params=pltpu.CompilerParams(collective_id=0, has_side_effects=True),
    )(own, weight)


def layer_kernel(
    n_sp, n_tp, capacity, groups,
    attended, out_weight, residual, gain, routes, routes_t, mix_w, w_gate, w_up, w_down,
    out,
    wg, wu, wd, p_in, after, n_out, n_in, x_out, x_all, act, y_out, y_in, y_own, y_keep, y_fwd, y_last,
    z_out, z_in,
    w_sem, p_send, p_recv, n_send, n_recv, x_send, x_recv, a_send, a_recv, r_send, r_recv,
    y_send, y_recv, e_send, e_recv, z_send, z_recv,
):
    me = lax.axis_index("sp")
    tp = lax.axis_index("tp")
    rows, cols = residual.shape
    hidden = w_gate.shape[1]
    square = n_tp == 4

    def to_tp(q):
        return tp_offset(tp, n_tp, q)

    def from_tp(q):
        return tp_origin(tp, n_tp, q)

    def to_sp(j):
        return lax.rem(me + j, n_sp)

    def from_sp(j):
        return lax.rem(me + n_sp - j, n_sp)

    def feats(t, width=cols, shift=0):
        return pl.ds(pl.multiple_of(t * cols + shift, 128), width)

    def block(j):
        return pl.ds(j * capacity, capacity)

    loads = [
        pltpu.make_async_copy(s, d, w_sem.at[i])
        for i, (s, d) in enumerate(((w_gate, wg), (w_up, wu), (w_down, wd)))
    ]
    for load in loads:
        load.start()

    barrier = pltpu.get_barrier_semaphore()
    for q in range(1, n_tp):
        pl.semaphore_signal(barrier, inc=1, device_id=(me, to_tp(q)), device_id_type=MESH)
    for j in range(1, n_sp):
        pl.semaphore_signal(barrier, inc=1, device_id=(to_sp(j), tp), device_id_type=MESH)
    pl.semaphore_wait(barrier, n_tp - 1 + n_sp - 1)

    order = [3, 1, 2] if square else list(range(1, n_tp))
    p_copies = {}
    for q in order:
        p_copies[q] = remote(attended, p_in.at[q], p_send.at[q], p_recv.at[q], me, to_tp(q))
        p_copies[q].start()
    total = dot(attended[...], out_weight[tp]).astype(BF16).astype(F32)

    tri = lax.broadcasted_iota(jnp.int32, (rows, rows), 0)
    tri_c = lax.broadcasted_iota(jnp.int32, (rows, rows), 1)
    upper = (tri < tri_c).astype(F32).astype(BF16)
    lower = (tri > tri_c).astype(F32).astype(BF16)
    expert_rows = lax.broadcasted_iota(jnp.int32, (n_sp, rows), 0)
    expert_cols = lax.broadcasted_iota(jnp.int32, (rows, n_sp), 1)
    hot_r = [(routes_t[k : k + 1, :] == expert_rows).astype(F32) for k in range(TOPK)]
    hot_c = [(routes[:, k : k + 1] == expert_cols).astype(F32) for k in range(TOPK)]
    before_r = dot(sum(hot_r).astype(BF16), upper)
    before_c = dot(lower, sum(hot_c).astype(BF16))
    slot_r, slot_c = [], []
    for k in range(TOPK):
        rank = jnp.sum(before_r * hot_r[k], axis=0, keepdims=True).astype(jnp.int32)
        rel = routes_t[k : k + 1, :] - me
        rel = jnp.where(rel < 0, rel + n_sp, rel)
        slot_r.append(rel * capacity + rank)
        rank = jnp.sum(before_c * hot_c[k], axis=1, keepdims=True).astype(jnp.int32)
        rel = routes[:, k : k + 1] - me
        rel = jnp.where(rel < 0, rel + n_sp, rel)
        slot_c.append(rel * capacity + rank)

    total = residual[...].astype(F32) + total
    for q in [1, 2, 3] if square else order:
        p_copies[q].wait_recv()
        total = total + dot(p_in[q], out_weight[from_tp(q)]).astype(BF16).astype(F32)
    after[...] = total
    square_sum = jnp.sum(total * total, axis=1, keepdims=True)
    as_rows = jnp.transpose(jnp.broadcast_to(square_sum, (rows, 128)))
    n_out[...] = as_rows[0:8, :]
    n_copies = []
    for q in range(1, n_tp):
        copy = remote(n_out, n_in.at[q], n_send.at[q], n_recv.at[q], me, to_tp(q))
        copy.start()
        n_copies.append(copy)
    sum_rows = n_out[...]
    for q in range(1, n_tp):
        n_copies[q - 1].wait_recv()
        sum_rows = sum_rows + n_in[q]
    all_sum = jnp.transpose(jnp.broadcast_to(sum_rows[0:1, :], (128, rows)))[:, 0:1]
    normed = (after[...] * lax.rsqrt(all_sum / D + norm_eps) * gain[...]).astype(BF16)

    x_copies = {}
    slot_id = lax.broadcasted_iota(jnp.int32, (capacity, rows), 0)
    for j in list(range(1, n_sp)) + [0]:
        ids = slot_id + j * capacity
        pick = ((ids == slot_r[0]) | (ids == slot_r[1])).astype(F32).astype(BF16)
        picked = dot(pick, normed).astype(BF16)
        x_out[j] = picked
        if j:
            x_copies[j] = remote(
                x_out.at[j], x_all.at[block(j), feats(tp)], x_send.at[j], x_recv.at[j], to_sp(j), tp
            )
            x_copies[j].start()
        else:
            x_all[block(0), feats(tp)] = picked

    direct = [1, 2] if square else list(range(1, n_tp))
    a_copies, r_copies = {}, {}

    def spread(j):
        if j:
            x_copies[j].wait_recv()
        part = x_all.at[block(j), feats(tp)]
        for q in direct:
            a_copies[q, j] = remote(part, part, a_send.at[q, j], a_recv.at[q, j], me, to_tp(q))
            a_copies[q, j].start()

    def await_direct(q, j):
        part = x_all.at[block(j), feats(from_tp(q))]
        remote(part, part, a_send.at[q, j], a_recv.at[q, j], me, to_tp(q)).wait_recv()

    def relay(j):
        half = cols // 2
        for i, q in enumerate((1, 2)):
            await_direct(q, j)
            part = x_all.at[block(j), feats(to_tp(q), half, i * half)]
            r_copies[i, j] = remote(part, part, r_send.at[i, j], r_recv.at[i, j], me, to_tp(3 - q))
            r_copies[i, j].start()

    def await_block(j):
        if square:
            half = cols // 2
            for i in range(2):
                part = x_all.at[block(j), feats(to_tp(3), half, i * half)]
                remote(part, part, r_send.at[i, j], r_recv.at[i, j], me, tp_peer).wait_recv()
        else:
            for q in direct:
                await_direct(q, j)

    tp_peer = to_tp(1)
    lag = 2
    for j in range(n_sp + lag):
        if j < n_sp:
            spread(j)
        if square and j >= lag:
            relay(j - lag)

    for load in loads:
        load.wait()
    per = n_sp // groups
    m = per * capacity
    tile = min(256, hidden)
    y_copies, e_copies, z_copies = {}, {}, {}
    half = cols // 2

    def send_parts(j):
        for i in range(2):
            at = (i, slice(None), block(j), slice(None))
            y_copies[i, j] = remote(
                y_out.at[at], y_in.at[at], y_send.at[i, j], y_recv.at[i, j], me, to_tp(1 + i)
            )
            y_copies[i, j].start()

    def pass_on(j):
        for i in range(2):
            y_copies[i, j].wait_recv()
            both = y_in[i, 0, block(j), :].astype(F32) + y_keep[i, block(j), :].astype(F32)
            y_fwd[i, block(j), :] = both.astype(BF16)
            at = (i, block(j), slice(None))
            e_copies[i, j] = remote(
                y_fwd.at[at], y_last.at[at], e_send.at[i, j], e_recv.at[i, j], me, to_tp(2 - i)
            )
            e_copies[i, j].start()

    def finish(j):
        if square:
            pieces = []
            for i in range(2):
                e_copies[i, j].wait_recv()
                piece = y_own[block(j), i * half : (i + 1) * half].astype(F32)
                piece = piece + y_in[i, 1, block(j), :].astype(F32)
                pieces.append((piece + y_last[i, block(j), :].astype(F32)).astype(BF16))
        else:
            acc = y_own[block(j), :].astype(F32)
            for q in range(1, n_tp):
                y_copies[q, j].wait_recv()
                acc = acc + y_in[q, block(j), :].astype(F32)
            pieces = [acc.astype(BF16)]
        width = cols // len(pieces)
        for i, piece in enumerate(pieces):
            at = slice(i * width, (i + 1) * width)
            if j == 0:
                z_in[0:capacity, at] = piece
            else:
                z_out[j, :, at] = piece
        if j:
            z_copies[j] = remote(
                z_out.at[j], z_in.at[block(j), :], z_send.at[j], z_recv.at[j], from_sp(j), tp
            )
            z_copies[j].start()

    for g in range(groups):
        for b in range(per):
            await_block(g * per + b)
        span = pl.ds(g * m, m)

        def hidden_tile(i, carry):
            at = pl.ds(pl.multiple_of(i * tile, 128), tile)
            gate = dot(x_all[span, :], wg[:, at])
            up = dot(x_all[span, :], wu[:, at])
            act[:, at] = (gate / (1.0 + jnp.exp(-gate)) * up).astype(BF16)
            return carry

        lax.fori_loop(0, hidden // tile, hidden_tile, 0)
        blocks = range(g * per, (g + 1) * per)
        if square:
            diag = dot(act[...], wd[:, feats(to_tp(3))]).astype(BF16)
            y_out[0, 0, span, :] = diag[:, :half]
            y_out[1, 0, span, :] = diag[:, half:]
            by_x = dot(act[...], wd[:, feats(to_tp(1))]).astype(BF16)
            y_out[0, 1, span, :] = by_x[:, :half]
            y_keep[1, span, :] = by_x[:, half:]
            by_y = dot(act[...], wd[:, feats(to_tp(2))]).astype(BF16)
            y_out[1, 1, span, :] = by_y[:, half:]
            y_keep[0, span, :] = by_y[:, :half]
            for j in blocks:
                send_parts(j)
        else:
            for q in order:
                y_out[q, span, :] = dot(act[...], wd[:, feats(to_tp(q))]).astype(BF16)
                for j in blocks:
                    at = (q, block(j), slice(None))
                    y_copies[q, j] = remote(
                        y_out.at[at], y_in.at[at], y_send.at[q, j], y_recv.at[q, j], me, to_tp(q)
                    )
                    y_copies[q, j].start()
        y_own[span, :] = dot(act[...], wd[:, feats(tp)]).astype(BF16)
    for j in range(n_sp + lag):
        if square and j < n_sp:
            pass_on(j)
        if j >= lag:
            finish(j - lag)

    slot_lane = lax.broadcasted_iota(jnp.int32, (rows, n_sp * capacity), 1)
    picks = [(slot_lane == slot_c[k]).astype(F32).astype(BF16) for k in range(TOPK)]
    for j in range(1, n_sp):
        z_copies[j].wait_recv()
    mix = dot(picks[0], z_in[...]) * mix_w[:, 0:1]
    mix = mix + dot(picks[1], z_in[...]) * mix_w[:, 1:2]
    out[...] = (after[...] + mix).astype(BF16)

    for copies in (p_copies, x_copies, a_copies, r_copies, y_copies, e_copies, z_copies):
        for copy in copies.values():
            copy.wait_send()
    for copy in n_copies:
        copy.wait_send()


def layer(
    n_sp, n_tp, attended, out_weight, residual, norm_gain, routes, route_weights,
    w_gate, w_up, w_down,
):
    rows, cols = residual.shape
    hidden = w_gate.shape[1]
    capacity = 5 * rows * TOPK // (4 * n_sp) + 1
    capacity = -(-capacity // ROW_TILE) * ROW_TILE
    groups = 2
    slots = n_sp * capacity
    square = n_tp == 4
    parts = (2, 2, slots, cols // 2) if square else (n_tp, slots, cols)
    relayed = (2, slots, cols // 2) if square else (2, 8, 128)
    dma = pltpu.SemaphoreType.DMA
    vmem = pl.BlockSpec(memory_space=VMEM)
    hbm = pl.BlockSpec(memory_space=pl.ANY)
    return pl.pallas_call(
        functools.partial(layer_kernel, n_sp, n_tp, capacity, groups),
        out_shape=jax.ShapeDtypeStruct((rows, cols), BF16),
        in_specs=[vmem] * 7 + [hbm] * 3,
        out_specs=vmem,
        scratch_shapes=[
            VMEM((D, hidden), BF16),
            VMEM((D, hidden), BF16),
            VMEM((hidden, D), BF16),
            VMEM((n_tp,) + attended.shape, BF16),
            VMEM((rows, cols), F32),
            VMEM((8, rows), F32),
            VMEM((n_tp, 8, rows), F32),
            VMEM((n_sp, capacity, cols), BF16),
            VMEM((slots, D), BF16),
            VMEM((slots // groups, hidden), BF16),
            VMEM(parts, BF16),
            VMEM(parts, BF16),
            VMEM((slots, cols), BF16),
            VMEM(relayed, BF16),
            VMEM(relayed, BF16),
            VMEM(relayed, BF16),
            VMEM((n_sp, capacity, cols), BF16),
            VMEM((slots, cols), BF16),
            dma((3,)),
            dma((n_tp,)), dma((n_tp,)),
            dma((n_tp,)), dma((n_tp,)),
            dma((n_sp,)), dma((n_sp,)),
            dma((n_tp, n_sp)), dma((n_tp, n_sp)),
            dma((2, n_sp)), dma((2, n_sp)),
            dma((n_tp, n_sp)), dma((n_tp, n_sp)),
            dma((2, n_sp)), dma((2, n_sp)),
            dma((n_sp,)), dma((n_sp,)),
        ],
        compiler_params=pltpu.CompilerParams(
            collective_id=1, has_side_effects=True, vmem_limit_bytes=60 * 1024 * 1024
        ),
    )(
        attended, out_weight, residual, norm_gain.reshape(1, cols), routes, routes.T,
        route_weights, w_gate, w_up, w_down,
    )


def shards(
    n_sp,
    n_tp,
    query_heads,
    key_heads,
    value_heads,
    q_gain,
    k_gain,
    out_weight,
    residual,
    norm_gain,
    routes,
    route_weights,
    w_gate,
    w_up,
    w_down,
):
    tok_rows = query_heads.shape[0]
    head_local = query_heads.shape[1] // E
    group_size = HQ // KV
    kv_count = max(head_local // group_size, 1)
    per_kv = head_local // kv_count
    tp_index = lax.axis_index("tp")
    sp_index = lax.axis_index("sp")
    kv_first = tp_index * head_local // group_size
    positions = sp_index * tok_rows + jnp.arange(tok_rows, dtype=jnp.int32)
    query_f = query_heads.astype(jnp.float32).reshape(tok_rows, kv_count, per_kv, E)
    q_turned = rotate(normalize(query_f, q_gain), positions).astype(jnp.bfloat16)
    key_cols = lax.dynamic_slice_in_dim(key_heads, kv_first * E, kv_count * E, 1)
    value_cols = lax.dynamic_slice_in_dim(value_heads, kv_first * E, kv_count * E, 1)
    key_f = key_cols.astype(jnp.float32).reshape(tok_rows, kv_count, E)
    k_turned = rotate(normalize(key_f, k_gain), positions).astype(jnp.bfloat16)
    width = kv_count * E
    own = jnp.concatenate([k_turned.reshape(tok_rows, width), value_cols], axis=1)
    both, out_weight = gather_kv(n_sp, n_tp, own, out_weight)
    both = both.reshape(n_sp * tok_rows, 2 * width)
    key_block = both[:, :width].reshape(-1, kv_count, E)
    value_block = both[:, width:].reshape(-1, kv_count, E)
    scores = jnp.einsum(
        "qcge,kce->cgqk", q_turned, key_block, preferred_element_type=jnp.float32
    ) * E ** (-0.5)
    new_max = jnp.max(scores, axis=-1)
    exped = jnp.exp(scores - new_max[..., None])
    denominator = jnp.sum(exped, axis=-1)
    weighted = jnp.einsum(
        "cgqk,kce->cgqe",
        exped.astype(jnp.bfloat16),
        value_block,
        preferred_element_type=jnp.float32,
    )
    attended = (weighted / denominator[..., None]).astype(jnp.bfloat16)
    attended = attended.transpose(2, 0, 1, 3).reshape(tok_rows, head_local * E)
    return layer(
        n_sp, n_tp, attended, out_weight, residual, norm_gain, routes, route_weights,
        w_gate[0], w_up[0], w_down[0],
    )


def flip(index, bits, size):
    mirrored = 0
    step = 1
    while step < size:
        digit = lax.rem(lax.div(index, step), 2)
        mirrored = mirrored + step * (1 - digit if bits & step else digit)
        step *= 2
    return mirrored


def swap_lanes(lanes, quarter):
    return jnp.where(jnp.bitwise_and(lanes, quarter) == 0, lanes + quarter, lanes - quarter)


def swap_quarters(gain, quarter):
    parts = [gain[:, i * quarter : (i + 1) * quarter] for i in (1, 0, 3, 2)]
    return jnp.concatenate(parts, axis=1)


def as_bf16(mask):
    return mask.astype(F32).astype(BF16)


def square_sums(values_f, same_head):
    squared = values_f * values_f
    high = squared.astype(BF16)
    low = (squared - high.astype(F32)).astype(BF16)
    return dot(high, same_head) + dot(low, same_head)


def fused_kernel(
    n_sp, n_tp, base, tail, chunks, order,
    weight, w_gate, w_up, w_down, *rest,
):
    small, out, staged, rest = rest[:10], rest[10], rest[11:21], rest[21:]
    query, keys, values, q_gain, k_gain, table, residual, gain, routes_t, mix_t = staged
    (
        wg, wu, wd, wo, own, kv, q_st, scores_st, top, probs, denom, att, pick_st, mixers,
        after, n_out, n_in, s_out, s_in, x_out, x_tail, x_all, act,
        y_out, y_in, y_own, y_keep, y_fwd, y_last, z_out, z_tail, z_in,
        l_sem, w_sem, o_send, o_recv, v_send, v_recv, k_send, k_recv, p_send, p_recv,
        n_send, n_recv, s_send, s_recv, x_send, x_recv, g_send, g_recv, a_send, a_recv, r_send, r_recv,
        y_send, y_recv, e_send, e_recv, z_send, z_recv, h_send, h_recv,
    ) = rest
    me = lax.axis_index("sp")
    tp = lax.axis_index("tp")
    rows, cols = out.shape
    hidden = wg.shape[1]
    features = cols * n_tp
    width = query.shape[1]
    heads = width // E
    chunk = rows // chunks
    stacked = heads * chunk
    groups = n_sp // 2
    pair = 2 * base
    extra = -(-n_sp * tail // 8) * 8
    cap = base + extra
    full = n_sp * base
    half = cols // 2
    core = lax.rem(me, 2)
    sp_peer = [flip(me, i, n_sp) for i in range(n_sp)]
    tp_peer = [flip(tp, q, n_tp) for q in range(n_tp)]
    sent = []

    def start(copy):
        copy.start()
        sent.append(copy)
        return copy

    def feats(q, size=cols, shift=0):
        return pl.ds(pl.multiple_of(tp_peer[q] * cols + shift, 128), size)

    def block(i):
        return pl.ds(i * base, base if i < n_sp else extra)

    barrier = pltpu.get_barrier_semaphore()
    for q in range(1, n_tp):
        pl.semaphore_signal(barrier, inc=1, device_id=(me, tp_peer[q]), device_id_type=MESH)
    for i in range(1, n_sp):
        pl.semaphore_signal(barrier, inc=1, device_id=(sp_peer[i], tp), device_id_type=MESH)
    fetches = [
        pltpu.make_async_copy(s, d, l_sem.at[i]) for i, (s, d) in enumerate(zip(small, staged))
    ]
    for i in (1, 2, 4, 5, 0, 3, 8, 9, 6, 7):
        fetches[i].start()
    own_cols = pltpu.make_async_copy(weight.at[:, feats(0)], wo.at[0], w_sem.at[3])
    own_cols.start()

    quarter = E // 4
    kv_first = lax.div(tp * heads * KV, HQ)
    source = lax.broadcasted_iota(jnp.int32, (keys.shape[1], 2 * E), 0) - kv_first * E
    lanes = lax.broadcasted_iota(jnp.int32, (keys.shape[1], 2 * E), 1)
    first = lanes < E
    for i in (1, 2, 4, 5):
        fetches[i].wait()
    k_f = dot(keys[...], as_bf16((source == lanes) & first))
    k_swap = dot(keys[...], as_bf16((source == swap_lanes(lanes, quarter)) & first))
    v_f = dot(values[...], as_bf16((source == lanes - E) & (lanes >= E)))
    grid_rows = rows // GRID_W
    all_rows = table.shape[0] - GRID_W
    by_col = table[all_rows:, :]
    turns = jnp.concatenate(
        [by_col + table[pl.ds(me * grid_rows + j, 1), :] for j in range(grid_rows)], axis=0
    )
    cosine, sine = turns[:, : 2 * E], turns[:, 2 * E :]
    gain_k = jnp.concatenate([k_gain[...]] * 2, axis=1)
    gain_ks = jnp.concatenate([swap_quarters(k_gain[...], quarter)] * 2, axis=1)
    sums = square_sums(k_f, jnp.ones((2 * E, 2 * E), BF16))
    k_turned = (k_f * gain_k) * cosine + (k_swap * gain_ks) * sine
    k_turned = k_turned * lax.rsqrt(sums / E + norm_eps)
    own[...] = (k_turned + v_f).astype(BF16)

    pl.semaphore_wait(barrier, n_tp - 1 + n_sp - 1)

    k_copies = {}
    for g in range(1, groups):
        k_copies[2 * g] = start(
            remote(own, kv.at[2 * g], k_send.at[2 * g], k_recv.at[2 * g], sp_peer[2 * g], tp)
        )
    k_copies[1] = start(remote(own, kv.at[1], k_send.at[1], k_recv.at[1], sp_peer[1], tp))
    depth = wo.shape[1] // 2
    mine = pl.ds(pl.multiple_of(core * depth, 16), depth)
    o_copies = {}
    for q in (3, 1, 2):
        o_copies[q] = start(
            remote(
                weight.at[mine, feats(q)], wo.at[q, mine, :], o_send.at[q], o_recv.at[q],
                me, tp_peer[q],
            )
        )
    loads = [
        pltpu.make_async_copy(s, d, w_sem.at[i])
        for i, (s, d) in enumerate(((w_gate, wg), (w_up, wu), (w_down, wd)))
    ]
    for load in loads:
        load.start()
    kv[0] = own[...]

    for i in (0, 3, 8, 9, 6, 7):
        fetches[i].wait()
    from_lane = lax.broadcasted_iota(jnp.int32, (width, width), 0)
    to_lane = lax.broadcasted_iota(jnp.int32, (width, width), 1)
    head_bits = width - E
    same = as_bf16(
        jnp.bitwise_and(from_lane, head_bits) == jnp.bitwise_and(to_lane, head_bits)
    )
    q_f = query[...].astype(F32)
    q_swap = dot(query[...], as_bf16(from_lane == swap_lanes(to_lane, quarter)))
    copies_of = width // (2 * E)
    gain_q = jnp.concatenate([q_gain[...]] * heads, axis=1)
    gain_qs = jnp.concatenate([swap_quarters(q_gain[...], quarter)] * heads, axis=1)
    q_turned = (q_f * gain_q) * jnp.concatenate([cosine] * copies_of, axis=1)
    q_turned = q_turned + (q_swap * gain_qs) * jnp.concatenate([sine] * copies_of, axis=1)
    q_turned = q_turned * lax.rsqrt(square_sums(q_f, same) / E + norm_eps)
    q_turned = (q_turned * E ** (-0.5)).astype(BF16)
    q_st[...] = jnp.zeros_like(q_st)
    for c in range(chunks):
        for h in range(heads):
            q_st[pl.ds((c * heads + h) * chunk, chunk), 0:E] = q_turned[
                c * chunk : (c + 1) * chunk, h * E : (h + 1) * E
            ]

    def score(i):
        at = pl.ds(i * rows, rows)

        def score_chunk(c, carry):
            span = pl.ds(pl.multiple_of(c * stacked, 16), stacked)
            s = lax.dot_general(
                q_st[span, :], kv[i], (((1,), (1,)), ((), ())), preferred_element_type=F32
            )
            scores_st[span, at] = s
            folded = s[:, 0:128]
            for lane in range(128, rows, 128):
                folded = jnp.maximum(folded, s[:, lane : lane + 128])
            top[span, :] = folded if i == 0 else jnp.maximum(top[span, :], folded)
            return carry

        lax.fori_loop(0, chunks, score_chunk, 0)

    def pass_kv(g):
        k_copies[2 * g].wait_recv()
        k_copies[2 * g + 1] = start(
            remote(
                kv.at[2 * g], kv.at[2 * g + 1], k_send.at[2 * g + 1], k_recv.at[2 * g + 1],
                sp_peer[1], tp,
            )
        )

    score(0)
    k_copies[1].wait_recv()
    score(1)

    before_id = lax.broadcasted_iota(jnp.int32, (rows, rows), 0)
    after_id = lax.broadcasted_iota(jnp.int32, (rows, rows), 1)
    expert_id = lax.broadcasted_iota(jnp.int32, (n_sp, rows), 0)
    hot = [(routes_t[k : k + 1, :] == expert_id).astype(F32) for k in range(TOPK)]
    before = dot(sum(hot).astype(BF16), as_bf16(before_id < after_id))
    ranks = [jnp.sum(before * h, axis=0, keepdims=True).astype(jnp.int32) for h in hot]
    slot_id = lax.broadcasted_iota(jnp.int32, (cap, rows), 0)
    slots_r = [jnp.zeros((1, rows), jnp.int32) for _ in range(TOPK)]
    for i in range(n_sp):
        here = [routes_t[k : k + 1, :] == sp_peer[i] for k in range(TOPK)]
        ids = [jnp.where(here[k], ranks[k], -1) for k in range(TOPK)]
        spare = jnp.where(
            (slot_id >= base + i * tail) & (slot_id < base + (i + 1) * tail), slot_id - i * tail, -2
        )
        rank_id = jnp.where(slot_id < base, slot_id, spare)
        pick_st[i * cap : (i + 1) * cap, :] = as_bf16((rank_id == ids[0]) | (rank_id == ids[1]))
        spot = [
            jnp.where(r < base, r + i * base, r - base + full + i * (extra + tail)) for r in ranks
        ]
        slots_r = [jnp.where(here[k], spot[k], slots_r[k]) for k in range(TOPK)]
    packed = jnp.concatenate(
        [s.astype(F32) for s in slots_r] + [mix_t[...], jnp.zeros((8 - 2 * TOPK, rows), F32)],
        axis=0,
    )
    packed = jnp.transpose(packed)
    slots_c = [packed[:, k : k + 1].astype(jnp.int32) for k in range(TOPK)]
    mix_c = [packed[:, TOPK + k : TOPK + k + 1] for k in range(TOPK)]
    slot_lane = lax.broadcasted_iota(jnp.int32, mixers.shape[2:], 1)
    for g in range(groups):
        for k in range(TOPK):
            mixers[g, k] = as_bf16(slot_lane == slots_c[k] - g * pair)

    for g in range(1, groups):
        pass_kv(g)
        score(2 * g)
        if g > 1:
            k_copies[2 * g - 1].wait_recv()
            score(2 * g - 1)
    for q in (1, 2, 3):
        o_copies[q].wait_recv()
        part = wo.at[q, mine, :]
        o_copies[q, "pair"] = start(
            remote(part, part, v_send.at[q], v_recv.at[q], sp_peer[1], tp)
        )
    k_copies[n_sp - 1].wait_recv()
    score(n_sp - 1)

    p_copies = {}
    for c in range(chunks):

        def head_probs(h, carry):
            span = pl.ds(pl.multiple_of(c * stacked + h * chunk, 16), chunk)
            dest = pl.ds(pl.multiple_of(h * chunk, 16), chunk)
            peak = jnp.max(top[span, :], axis=1, keepdims=True)
            total = jnp.zeros((chunk, 128), F32)
            for lane in range(0, n_sp * rows, 256):
                p = jnp.exp(scores_st[span, lane : lane + 256] - peak)
                probs[dest, lane : lane + 256] = p.astype(BF16)
                total = total + p[:, 0:128] + p[:, 128:256]
            total = jnp.sum(total, axis=1, keepdims=True)
            denom[dest, :] = jnp.broadcast_to(total, (chunk, 128))
            return carry

        lax.fori_loop(0, heads, head_probs, 0)
        values_all = kv[...].reshape(n_sp * rows, 2 * E)
        weighted = dot(probs[...], values_all)[:, E:] / denom[:, 0:E]
        weighted = weighted.astype(BF16)
        att[0, c] = jnp.concatenate(
            [weighted[h * chunk : (h + 1) * chunk, :] for h in range(heads)], axis=1
        )
        for q in (3, 1, 2):
            p_copies[q, c] = start(
                remote(
                    att.at[0, c], att.at[q, c], p_send.at[q, c], p_recv.at[q, c], me, tp_peer[q]
                )
            )

    own_cols.wait()
    for q in (1, 2, 3):
        o_copies[q, "pair"].wait_recv()
    for c in range(chunks):
        at = slice(c * chunk, (c + 1) * chunk)
        total = residual[at, :].astype(F32) + dot(att[0, c], wo[0]).astype(BF16).astype(F32)
        for q in (1, 2, 3):
            p_copies[q, c].wait_recv()
            total = total + dot(att[q, c], wo[q]).astype(BF16).astype(F32)
        after[at, :] = total
    total = after[...]
    square_sum = jnp.sum(total * total, axis=1, keepdims=True)
    n_out[...] = jnp.transpose(jnp.broadcast_to(square_sum, (rows, 128)))[0:8, :]
    n_copies = {}
    for q in (3, 1, 2):
        n_copies[q] = start(
            remote(n_out, n_in.at[q], n_send.at[q], n_recv.at[q], me, tp_peer[q])
        )
    scaled = (total * gain[...]).astype(BF16)

    x_copies, a_copies, r_copies, s_copies = {}, {}, {}, {}
    y_copies, e_copies, z_copies = {}, {}, {}

    def spread(i):
        if i == n_sp:
            gathered = x_tail[0].astype(F32)
            for j in range(1, n_sp):
                x_copies[j, "tail"].wait_recv()
                gathered = gathered + x_tail[j].astype(F32)
            x_all[block(i), feats(0)] = gathered.astype(BF16)
        elif i:
            x_copies[i].wait_recv()
        part = x_all.at[block(i), feats(0)]
        for q in (1, 2):
            a_copies[q, i] = start(
                remote(part, part, a_send.at[q, i], a_recv.at[q, i], me, tp_peer[q])
            )

    def relay(i):
        for q in (1, 2):
            whole = x_all.at[block(i), feats(q)]
            remote(whole, whole, a_send.at[q, i], a_recv.at[q, i], me, tp_peer[q]).wait_recv()
            part = x_all.at[block(i), feats(q, half, (q - 1) * half)]
            r_copies[q, i] = start(
                remote(part, part, r_send.at[q, i], r_recv.at[q, i], me, tp_peer[3 - q])
            )

    def await_block(i):
        for q in (1, 2):
            part = x_all.at[block(i), feats(3, half, (q - 1) * half)]
            remote(part, part, r_send.at[q, i], r_recv.at[q, i], me, tp_peer[3 - q]).wait_recv()

    def send_picked(i):
        picked = dot(pick_st[i * cap : (i + 1) * cap, :], scaled).astype(BF16)
        if i:
            x_out[i] = picked
            x_copies[i] = start(
                remote(
                    x_out.at[i, 0:base, :], x_all.at[block(i), feats(0)], x_send.at[i],
                    x_recv.at[i], sp_peer[i], tp,
                )
            )
            x_copies[i, "tail"] = start(
                remote(
                    x_out.at[i, base:cap, :], x_tail.at[i], g_send.at[i], g_recv.at[i],
                    sp_peer[i], tp,
                )
            )
        else:
            x_all[block(0), feats(0)] = picked[0:base]
            x_tail[0] = picked[base:cap]

    def send_scales(_):
        sum_rows = n_out[...]
        for q in (1, 2, 3):
            n_copies[q].wait_recv()
            sum_rows = sum_rows + n_in[q]
        scale_c = jnp.transpose(lax.rsqrt(sum_rows / features + norm_eps))[:, 0:1]
        lane = lax.broadcasted_iota(jnp.int32, (rows, 128), 1)
        for i in range(n_sp):
            spot = jnp.where(lane < base, lane + i * base, lane - base + full + i * extra)
            here = (spot == slots_c[0]) | (spot == slots_c[1])
            row = jnp.sum(jnp.where(here, scale_c, 0.0), axis=0, keepdims=True)
            tile = jnp.broadcast_to(row, (8, 128))
            if i:
                s_out[i] = tile
                s_copies[i] = start(
                    remote(s_out.at[i], s_in.at[i], s_send.at[i], s_recv.at[i], sp_peer[i], tp)
                )
            else:
                s_in[0] = tile

    tile = min(256, hidden)
    scaled_by = {0}

    def scales_of(i):
        if i not in scaled_by:
            s_copies[i].wait_recv()
            scaled_by.add(i)
        return s_in[i]

    def compute(g):
        members = [2 * g, 2 * g + 1]
        scale = [jnp.transpose(scales_of(i))[0:base, 0:1] for i in members]
        size = pair
        if g == groups - 1:
            tails = sum(scales_of(i) for i in range(n_sp))
            scale.append(jnp.transpose(tails)[base:cap, 0:1])
            members.append(n_sp)
            size = pair + extra
        scale = jnp.concatenate(scale, axis=0)
        for i in members:
            await_block(i)
        span = pl.ds(g * pair, size)
        used = pl.ds(0, size)

        def hidden_tile(t, carry):
            at = pl.ds(pl.multiple_of(t * tile, 128), tile)
            gate = dot(x_all[span, :], wg[:, at]) * scale
            up = dot(x_all[span, :], wu[:, at]) * scale
            act[used, at] = (gate / (1.0 + jnp.exp(-gate)) * up).astype(BF16)
            return carry

        lax.fori_loop(0, hidden // tile, hidden_tile, 0)
        diag = dot(act[used, :], wd[:, feats(3)]).astype(BF16)
        y_out[0, 0, span, :] = diag[:, :half]
        y_out[1, 0, span, :] = diag[:, half:]
        by_x = dot(act[used, :], wd[:, feats(1)]).astype(BF16)
        y_out[0, 1, span, :] = by_x[:, :half]
        y_keep[1, span, :] = by_x[:, half:]
        by_y = dot(act[used, :], wd[:, feats(2)]).astype(BF16)
        y_out[1, 1, span, :] = by_y[:, half:]
        y_keep[0, span, :] = by_y[:, :half]
        y_own[span, :] = dot(act[used, :], wd[:, feats(0)]).astype(BF16)

    def send_parts(i):
        for h in range(2):
            at = (h, slice(None), block(i), slice(None))
            y_copies[h, i] = start(
                remote(
                    y_out.at[at], y_in.at[at], y_send.at[h, i], y_recv.at[h, i], me, tp_peer[1 + h]
                )
            )

    def pass_on(i):
        for h in range(2):
            y_copies[h, i].wait_recv()
            both = y_in[h, 0, block(i), :].astype(F32) + y_keep[h, block(i), :].astype(F32)
            y_fwd[h, block(i), :] = both.astype(BF16)
            at = (h, block(i), slice(None))
            e_copies[h, i] = start(
                remote(
                    y_fwd.at[at], y_last.at[at], e_send.at[h, i], e_recv.at[h, i], me, tp_peer[2 - h]
                )
            )

    def finish(i):
        for h in range(2):
            e_copies[h, i].wait_recv()
            at = slice(h * half, (h + 1) * half)
            piece = y_own[block(i), at].astype(F32) + y_in[h, 1, block(i), :].astype(F32)
            piece = (piece + y_last[h, block(i), :].astype(F32)).astype(BF16)
            if i == n_sp:
                z_tail[:, at] = piece
                z_in[full : full + extra, at] = piece
            elif i:
                z_out[i, :, at] = piece
            else:
                z_in[0:base, at] = piece
        if i == n_sp:
            for j in range(1, n_sp):
                z_copies[j, "tail"] = start(
                    remote(
                        z_tail, z_in.at[pl.ds(full + j * extra, extra), :], h_send.at[j],
                        h_recv.at[j], sp_peer[j], tp,
                    )
                )
        elif i:
            z_copies[i] = start(
                remote(
                    z_out.at[i], z_in.at[block(i), :], z_send.at[i], z_recv.at[i], sp_peer[i], tp
                )
            )

    def mixed(g):
        for i in (2 * g, 2 * g + 1):
            if i:
                z_copies[i].wait_recv()
        size = pair
        if g == groups - 1:
            for j in range(1, n_sp):
                z_copies[j, "tail"].wait_recv()
            size = pair + n_sp * extra
        total = after[...]
        for k in range(TOPK):
            gathered = dot(mixers[g, k, :, 0:size], z_in[g * pair : g * pair + size, :])
            total = total + gathered * mix_c[k]
        return total

    def mix(g):
        after[...] = mixed(g)

    def mix_last(_):
        out[...] = mixed(0)

    def await_weights(_):
        for load in loads:
            load.wait()

    steps = {
        "X": send_picked, "S": spread, "R": relay, "N": send_scales, "W": await_weights,
        "C": compute, "Y": send_parts, "P": pass_on, "F": finish, "M": mix, "E": mix_last,
    }
    for step in order:
        steps[step[0]](int(step[1:] or 0))

    for copy in sent:
        copy.wait_send()


def turn_table(tokens):
    quarter = E // 4
    frequency = (rope_base ** (-np.arange(quarter) / quarter)).astype(np.float32)
    grid_rows = tokens // GRID_W

    def lanes_of(count, first):
        angles = np.arange(count, dtype=np.float32)[:, None] * frequency[None, :]
        blank = np.zeros((count, 2 * quarter), np.float32)
        cosine = np.concatenate([np.cos(angles)] * 2, axis=1)
        sines = np.concatenate([-np.sin(angles), np.sin(angles)], axis=1)
        both = []
        for part in (cosine, sines):
            head = [part, blank] if first else [blank, part]
            both += head * 2
        return np.concatenate(both, axis=1)

    return np.concatenate([lanes_of(grid_rows, True), lanes_of(GRID_W, False)], axis=0)


ORDER = (
    "X4", "X2", "X0", "X1", "S0", "S1", "R0", "X5", "S2", "X3", "S4", "X6", "R1", "S5", "N", "W",
    "S3", "R4", "X7", "R5", "S6", "R2", "C0", "S7", "R3", "S8", "C2", "Y5", "Y4", "R7", "R6",
    "R8", "C1", "Y2", "P5", "Y3", "P4", "C3", "F5", "P2", "Y7", "Y8", "Y6", "F2", "F4", "P3",
    "P7", "P8", "P6", "Y1", "Y0", "F7", "F8", "F3", "M2", "P1", "F6", "P0", "F1", "M1", "M3",
    "F0", "E",
)


def fused_shards(
    n_sp,
    n_tp,
    query_heads,
    key_heads,
    value_heads,
    q_gain,
    k_gain,
    out_weight,
    residual,
    norm_gain,
    routes,
    route_weights,
    w_gate,
    w_up,
    w_down,
):
    rows, cols = residual.shape
    width = query_heads.shape[1]
    heads = width // E
    hidden = w_gate.shape[2]
    features = cols * n_tp
    cap = 5 * rows * TOPK // (4 * n_sp) + 1
    tail = cap % ROW_TILE or ROW_TILE
    base = cap - tail
    extra = -(-n_sp * tail // ROW_TILE) * ROW_TILE
    cap = base + extra
    slots = n_sp * base + extra
    pair = 2 * base
    half = cols // 2
    chunks = 4
    chunk = rows // chunks
    dma = pltpu.SemaphoreType.DMA
    vmem = pl.BlockSpec(memory_space=VMEM)
    hbm = pl.BlockSpec(memory_space=pl.ANY)
    table = jnp.asarray(turn_table(n_sp * rows))
    small = (
        query_heads, key_heads, value_heads, q_gain.reshape(1, E), k_gain.reshape(1, E), table,
        residual, norm_gain.reshape(1, cols), routes.T, route_weights.T,
    )
    total = pl.pallas_call(
        functools.partial(fused_kernel, n_sp, n_tp, base, tail, chunks, ORDER),
        out_shape=jax.ShapeDtypeStruct((rows, cols), F32),
        in_specs=[hbm] * (4 + len(small)),
        out_specs=vmem,
        scratch_shapes=[VMEM(array.shape, array.dtype) for array in small] + [
            VMEM((features, hidden), BF16),
            VMEM((features, hidden), BF16),
            VMEM((hidden, features), BF16),
            VMEM((n_tp, width, cols), BF16),
            VMEM((rows, 2 * E), BF16),
            VMEM((n_sp, rows, 2 * E), BF16),
            VMEM((heads * rows, 2 * E), BF16),
            VMEM((heads * rows, n_sp * rows), F32),
            VMEM((heads * rows, 128), F32),
            VMEM((heads * chunk, n_sp * rows), BF16),
            VMEM((heads * chunk, 128), F32),
            VMEM((n_tp, chunks, chunk, width), BF16),
            VMEM((n_sp * cap, rows), BF16),
            VMEM((n_sp // 2, TOPK, rows, pair + n_sp * extra), BF16),
            VMEM((rows, cols), F32),
            VMEM((8, rows), F32),
            VMEM((n_tp, 8, rows), F32),
            VMEM((n_sp, 8, 128), F32),
            VMEM((n_sp, 8, 128), F32),
            VMEM((n_sp, cap, cols), BF16),
            VMEM((n_sp, extra, cols), BF16),
            VMEM((slots, features), BF16),
            VMEM((pair + extra, hidden), BF16),
            VMEM((2, 2, slots, half), BF16),
            VMEM((2, 2, slots, half), BF16),
            VMEM((slots, cols), BF16),
            VMEM((2, slots, half), BF16),
            VMEM((2, slots, half), BF16),
            VMEM((2, slots, half), BF16),
            VMEM((n_sp, base, cols), BF16),
            VMEM((extra, cols), BF16),
            VMEM((n_sp * cap, cols), BF16),
            dma((len(small),)),
            dma((4,)),
            dma((n_tp,)), dma((n_tp,)),
            dma((n_tp,)), dma((n_tp,)),
            dma((n_sp,)), dma((n_sp,)),
            dma((n_tp, chunks)), dma((n_tp, chunks)),
            dma((n_tp,)), dma((n_tp,)),
            dma((n_sp,)), dma((n_sp,)),
            dma((n_sp,)), dma((n_sp,)),
            dma((n_sp,)), dma((n_sp,)),
            dma((3, n_sp + 1)), dma((3, n_sp + 1)),
            dma((3, n_sp + 1)), dma((3, n_sp + 1)),
            dma((2, n_sp + 1)), dma((2, n_sp + 1)),
            dma((2, n_sp + 1)), dma((2, n_sp + 1)),
            dma((n_sp,)), dma((n_sp,)),
            dma((n_sp,)), dma((n_sp,)),
        ],
        compiler_params=pltpu.CompilerParams(
            collective_id=2, has_side_effects=True, vmem_limit_bytes=60 * 1024 * 1024
        ),
    )(out_weight, w_gate[0], w_up[0], w_down[0], *small)
    return total.astype(BF16)


def solution(mesh):
    n_sp, n_tp = mesh.shape["sp"], mesh.shape["tp"]
    local = fused_shards if n_tp == 4 and n_sp == 8 else shards
    return jax.shard_map(
        functools.partial(local, n_sp, n_tp),
        mesh=mesh,
        in_specs=(
            P("sp", "tp"),
            P("sp", None),
            P("sp", None),
            P(),
            P(),
            P("tp", None),
            P("sp", "tp"),
            P("tp"),
            P("sp", None),
            P("sp", None),
            P("sp", None, "tp"),
            P("sp", None, "tp"),
            P("sp", "tp", None),
        ),
        out_specs=P("sp", "tp"),
        check_vma=False,
    )
```

profile of v0, /device:TPU:0, one launch (start us, length us, event | category | flops | bytes accessed | tf_op | source)
XLA Modules:
  0.0 80.2 jit_solution(7923454516262373709)
XLA Ops:
  0.0 78.5 %shard_map.136 = f32[256,512]{1,0:T(8,128)} custom-call(bf16[256,2048]{1,0:T(8,128)(2,1)} %weight.1, bf16[2048,1024]{1,0:T(8,128)(2,1)} %bitcast.8, bf16[2048,1024]{1,0:T(8,128)(2,1)} %bitcast.9, bf16[1024,2048]{1,0:T(8,128)(2,1)} %bitcast.10, bf16[256,256]{1,0:T(8,128)(2,1)} %rest_0_.1, bf16[256,256]{1,0:T(8,128)(2,1)} %rest_1_.1, ...), custom_call_target="tpu_custom_call" | custom-call | tf_op jit(solution)/shard_map/pallas_call | solution.py:1089
  78.5 1.8 %convert_element_type.3 = bf16[256,512]{1,0:T(8,128)(2,1)} convert(f32[256,512]{1,0:T(8,128)} %shard_map.136) | non-fusion elementwise | flops 131072 | bytes 786432 | tf_op jit(solution)/shard_map/convert_element_type | solution.py:1148
where the time goes:
time: 80.4 us; the launch traced here: 80.2 us
  Pallas kernels  78.5 us (98%)
  other arithmetic  1.78 us (2%)
    pallas_call x1, Pallas kernels, fused_shards(): pl.pallas_call(functools.partial(fused_kernel, n_sp, n_tp, base, tail, ch...  78.5 us
    convert_element_type x1, other arithmetic, fused_shards(): return total.astype(BF16)  1.78 us

commit v1 on v0

--- a/solution.py
+++ b/solution.py
@@ -567,7 +567,7 @@
     query, keys, values, q_gain, k_gain, table, residual, gain, routes_t, mix_t = staged
     (
         wg, wu, wd, wo, own, kv, q_st, scores_st, top, probs, denom, att, pick_st, mixers,
-        after, n_out, n_in, s_out, s_in, x_out, x_tail, x_all, act,
+        scaled, after, n_out, n_in, s_out, s_in, x_out, x_tail, x_all, act,
         y_out, y_in, y_own, y_keep, y_fwd, y_last, z_out, z_tail, z_in,
         l_sem, w_sem, o_send, o_recv, v_send, v_recv, k_send, k_recv, p_send, p_recv,
         n_send, n_recv, s_send, s_recv, x_send, x_recv, g_send, g_recv, a_send, a_recv, r_send, r_recv,
@@ -695,7 +695,7 @@
         at = pl.ds(i * rows, rows)
 
         def score_chunk(c, carry):
-            span = pl.ds(pl.multiple_of(c * stacked, 16), stacked)
+            span = pl.ds(pl.multiple_of(c * rows, 16), rows)
             s = lax.dot_general(
                 q_st[span, :], kv[i], (((1,), (1,)), ((), ())), preferred_element_type=F32
             )
@@ -706,7 +706,7 @@
             top[span, :] = folded if i == 0 else jnp.maximum(top[span, :], folded)
             return carry
 
-        lax.fori_loop(0, chunks, score_chunk, 0)
+        lax.fori_loop(0, heads, score_chunk, 0)
 
     def pass_kv(g):
         k_copies[2 * g].wait_recv()
@@ -768,25 +768,23 @@
     k_copies[n_sp - 1].wait_recv()
     score(n_sp - 1)
 
+    peaks = jnp.max(top[...], axis=1, keepdims=True)
+    top[...] = jnp.broadcast_to(peaks, top.shape)
     p_copies = {}
     for c in range(chunks):
-
-        def head_probs(h, carry):
-            span = pl.ds(pl.multiple_of(c * stacked + h * chunk, 16), chunk)
-            dest = pl.ds(pl.multiple_of(h * chunk, 16), chunk)
-            peak = jnp.max(top[span, :], axis=1, keepdims=True)
+        for h in range(heads):
+            span = pl.ds(c * stacked + h * chunk, chunk)
+            dest = pl.ds(h * chunk, chunk)
+            peak = top[span, :]
             total = jnp.zeros((chunk, 128), F32)
-            for lane in range(0, n_sp * rows, 256):
-                p = jnp.exp(scores_st[span, lane : lane + 256] - peak)
-                probs[dest, lane : lane + 256] = p.astype(BF16)
-                total = total + p[:, 0:128] + p[:, 128:256]
-            total = jnp.sum(total, axis=1, keepdims=True)
-            denom[dest, :] = jnp.broadcast_to(total, (chunk, 128))
-            return carry
-
-        lax.fori_loop(0, heads, head_probs, 0)
+            for lane in range(0, n_sp * rows, 128):
+                p = jnp.exp(scores_st[span, lane : lane + 128] - peak)
+                probs[dest, lane : lane + 128] = p.astype(BF16)
+                total = total + p
+            denom[dest, :] = total
         values_all = kv[...].reshape(n_sp * rows, 2 * E)
-        weighted = dot(probs[...], values_all)[:, E:] / denom[:, 0:E]
+        weighted = dot(probs[...], values_all)[:, E:]
+        weighted = weighted / jnp.sum(denom[...], axis=1, keepdims=True)
         weighted = weighted.astype(BF16)
         att[0, c] = jnp.concatenate(
             [weighted[h * chunk : (h + 1) * chunk, :] for h in range(heads)], axis=1
@@ -803,20 +801,13 @@
         o_copies[q, "pair"].wait_recv()
     for c in range(chunks):
         at = slice(c * chunk, (c + 1) * chunk)
-        total = residual[at, :].astype(F32) + dot(att[0, c], wo[0]).astype(BF16).astype(F32)
         for q in (1, 2, 3):
             p_copies[q, c].wait_recv()
+        total = residual[at, :].astype(F32)
+        for q in range(n_tp):
             total = total + dot(att[q, c], wo[q]).astype(BF16).astype(F32)
         after[at, :] = total
-    total = after[...]
-    square_sum = jnp.sum(total * total, axis=1, keepdims=True)
-    n_out[...] = jnp.transpose(jnp.broadcast_to(square_sum, (rows, 128)))[0:8, :]
-    n_copies = {}
-    for q in (3, 1, 2):
-        n_copies[q] = start(
-            remote(n_out, n_in.at[q], n_send.at[q], n_recv.at[q], me, tp_peer[q])
-        )
-    scaled = (total * gain[...]).astype(BF16)
+        scaled[at, :] = (total * gain[...]).astype(BF16)
 
     x_copies, a_copies, r_copies, s_copies = {}, {}, {}, {}
     y_copies, e_copies, z_copies = {}, {}, {}
@@ -851,7 +842,7 @@
             remote(part, part, r_send.at[q, i], r_recv.at[q, i], me, tp_peer[3 - q]).wait_recv()
 
     def send_picked(i):
-        picked = dot(pick_st[i * cap : (i + 1) * cap, :], scaled).astype(BF16)
+        picked = dot(pick_st[i * cap : (i + 1) * cap, :], scaled[...]).astype(BF16)
         if i:
             x_out[i] = picked
             x_copies[i] = start(
@@ -869,6 +860,17 @@
         else:
             x_all[block(0), feats(0)] = picked[0:base]
             x_tail[0] = picked[base:cap]
+
+    n_copies = {}
+
+    def send_sums(_):
+        total = after[...]
+        square_sum = jnp.sum(total * total, axis=1, keepdims=True)
+        n_out[...] = jnp.transpose(jnp.broadcast_to(square_sum, (rows, 128)))[0:8, :]
+        for q in (3, 1, 2):
+            n_copies[q] = start(
+                remote(n_out, n_in.at[q], n_send.at[q], n_recv.at[q], me, tp_peer[q])
+            )
 
     def send_scales(_):
         sum_rows = n_out[...]
@@ -899,20 +901,21 @@
             scaled_by.add(i)
         return s_in[i]
 
-    def compute(g):
+    def size_of(g):
+        return pair + extra if g == groups - 1 else pair
+
+    def gate_up(g):
         members = [2 * g, 2 * g + 1]
         scale = [jnp.transpose(scales_of(i))[0:base, 0:1] for i in members]
-        size = pair
         if g == groups - 1:
             tails = sum(scales_of(i) for i in range(n_sp))
             scale.append(jnp.transpose(tails)[base:cap, 0:1])
             members.append(n_sp)
-            size = pair + extra
         scale = jnp.concatenate(scale, axis=0)
         for i in members:
             await_block(i)
-        span = pl.ds(g * pair, size)
-        used = pl.ds(0, size)
+        span = pl.ds(g * pair, size_of(g))
+        used = pl.ds(0, size_of(g))
 
         def hidden_tile(t, carry):
             at = pl.ds(pl.multiple_of(t * tile, 128), tile)
@@ -922,6 +925,10 @@
             return carry
 
         lax.fori_loop(0, hidden // tile, hidden_tile, 0)
+
+    def down(g):
+        span = pl.ds(g * pair, size_of(g))
+        used = pl.ds(0, size_of(g))
         diag = dot(act[used, :], wd[:, feats(3)]).astype(BF16)
         y_out[0, 0, span, :] = diag[:, :half]
         y_out[1, 0, span, :] = diag[:, half:]
@@ -1009,7 +1016,7 @@
 
     steps = {
         "X": send_picked, "S": spread, "R": relay, "N": send_scales, "W": await_weights,
-        "C": compute, "Y": send_parts, "P": pass_on, "F": finish, "M": mix, "E": mix_last,
+        "Q": send_sums, "G": gate_up, "D": down, "Y": send_parts, "P": pass_on, "F": finish, "M": mix, "E": mix_last,
     }
     for step in order:
         steps[step[0]](int(step[1:] or 0))
@@ -1038,11 +1045,11 @@
 
 
 ORDER = (
-    "X4", "X2", "X0", "X1", "S0", "S1", "R0", "X5", "S2", "X3", "S4", "X6", "R1", "S5", "N", "W",
-    "S3", "R4", "X7", "R5", "S6", "R2", "C0", "S7", "R3", "S8", "C2", "Y5", "Y4", "R7", "R6",
-    "R8", "C1", "Y2", "P5", "Y3", "P4", "C3", "F5", "P2", "Y7", "Y8", "Y6", "F2", "F4", "P3",
-    "P7", "P8", "P6", "Y1", "Y0", "F7", "F8", "F3", "M2", "P1", "F6", "P0", "F1", "M1", "M3",
-    "F0", "E",
+    "X4", "X0", "S0", "X2", "X1", "S1", "Q", "R0", "X5", "S2", "X3", "S4", "X6", "R1", "S5", "N",
+    "W", "S3", "R4", "X7", "R5", "S6", "R2", "G0", "D0", "S7", "R3", "S8", "G2", "D2", "R6", "Y5",
+    "Y4", "R7", "R8", "G1", "D1", "P5", "P4", "Y2", "Y3", "G3", "D3", "F5", "F4", "P2", "Y7",
+    "Y8", "Y6", "F2", "P3", "P7", "P8", "P6", "Y1", "Y0", "F7", "F8", "F3", "M2", "P1", "F6",
+    "P0", "F1", "M1", "M3", "F0", "E",
 )
 
 
@@ -1076,7 +1083,7 @@
     slots = n_sp * base + extra
     pair = 2 * base
     half = cols // 2
-    chunks = 4
+    chunks = 8
     chunk = rows // chunks
     dma = pltpu.SemaphoreType.DMA
     vmem = pl.BlockSpec(memory_space=VMEM)
@@ -1106,6 +1113,7 @@
             VMEM((n_tp, chunks, chunk, width), BF16),
             VMEM((n_sp * cap, rows), BF16),
             VMEM((n_sp // 2, TOPK, rows, pair + n_sp * extra), BF16),
+            VMEM((rows, cols), BF16),
             VMEM((rows, cols), F32),
             VMEM((8, rows), F32),
             VMEM((n_tp, 8, rows), F32),

time: 80.4 us -> 79 us (0.983)
  Pallas kernels: 78.5 us -> 77 us
    pallas_call x1, Pallas kernels: 78.5 us -> 77 us  [fused_shards(): pl.pallas_call(functools.partial(fused_kernel, n_sp, n_tp, base, tail, ch...]
where the time goes in v1:
time: 79 us; the launch traced here: 78.8 us
  Pallas kernels  77 us (97%)
  other arithmetic  1.78 us (2%)
    pallas_call x1, Pallas kernels, fused_shards(): pl.pallas_call(functools.partial(fused_kernel, n_sp, n_tp, base, tail, ch...  77 us
    convert_element_type x1, other arithmetic, fused_shards(): return total.astype(BF16)  1.78 us

profile of v1, /device:TPU:0, one launch (start us, length us, event | category | flops | bytes accessed | tf_op | source)
XLA Modules:
  0.0 78.8 jit_solution(13012741866207366786)
XLA Ops:
  0.0 77.0 %shard_map.136 = f32[256,512]{1,0:T(8,128)} custom-call(bf16[256,2048]{1,0:T(8,128)(2,1)} %weight.1, bf16[2048,1024]{1,0:T(8,128)(2,1)} %bitcast.8, bf16[2048,1024]{1,0:T(8,128)(2,1)} %bitcast.9, bf16[1024,2048]{1,0:T(8,128)(2,1)} %bitcast.10, bf16[256,256]{1,0:T(8,128)(2,1)} %rest_0_.1, bf16[256,256]{1,0:T(8,128)(2,1)} %rest_1_.1, ...), custom_call_target="tpu_custom_call" | custom-call | tf_op jit(solution)/shard_map/pallas_call | solution.py:1096
  77.1 1.8 %convert_element_type.3 = bf16[256,512]{1,0:T(8,128)(2,1)} convert(f32[256,512]{1,0:T(8,128)} %shard_map.136) | non-fusion elementwise | flops 131072 | bytes 786432 | tf_op jit(solution)/shard_map/convert_element_type | solution.py:1156
